TPU v7x, 32 devices: a whole 2x2x4 slice. The times are simulated.
32 devices in a mesh: ep: 8 (over z, y), tp: 4 (over x, core).
Axes of the slice: x: 2, y: 2, z: 4, core: 2. Of those that a mesh axis runs over, the one named last changes fastest.
Arguments:
- tokens: bfloat16 [128, 1024], P('ep', 'tp'), may hold values from -75 to 75
- gain_mix: float32 [1024], replicated, may hold values from 0.1 to 1.9
- w_query: bfloat16 [1024, 512], P(None, 'tp'), may hold values from -0.1875 to 0.1875
- w_key: bfloat16 [1024, 512], P(None, 'tp'), may hold values from -0.1875 to 0.1875
- w_value: bfloat16 [1024, 512], P(None, 'tp'), may hold values from -0.1875 to 0.1875
- w_outgate: bfloat16 [1024, 512], P(None, 'tp'), may hold values from -0.1875 to 0.1875
- w_input_gate: bfloat16 [1024, 4], P(None, 'tp'), may hold values from -0.1875 to 0.1875
- w_forget_gate: bfloat16 [1024, 4], P(None, 'tp'), may hold values from -0.1875 to 0.1875
- w_mix_out: bfloat16 [512, 1024], P(None, 'tp'), may hold values from -0.25 to 0.25
- cell_state: float32 [128, 4, 128, 128], P('ep', 'tp'), may hold values from -3 to 3
- norm_state: float32 [128, 4, 128], P('ep', 'tp'), may hold values from -3 to 3
- max_state: float32 [128, 4], P('ep', 'tp'), may hold values from -2 to 143
- gain_ffn: float32 [1024], replicated, may hold values from 0.1 to 1.9
- route_ids: int32 [128, 2], P('ep'), may hold values from 0 to 7, all different within a row; in each aligned block of 16 rows (0 to 15, 16 to 31, ...) at most 8 rows name the same one
- route_logits: float32 [128, 2], P('ep'), may hold values from -5 to 5
- expert_gate: bfloat16 [8, 1024, 1408], P('ep', None, 'tp'), may hold values from -0.1875 to 0.1875
- expert_up: bfloat16 [8, 1024, 1408], P('ep', None, 'tp'), may hold values from -0.1875 to 0.1875
- expert_down: bfloat16 [8, 1408, 1024], P('ep', 'tp'), may hold values from -0.15625 to 0.15625
- dense_gate: bfloat16 [1024, 3072], P('tp', 'ep'), may hold values from -0.1875 to 0.1875
- dense_up: bfloat16 [1024, 3072], P('tp', 'ep'), may hold values from -0.1875 to 0.1875
- dense_down: bfloat16 [3072, 1024], P('ep', 'tp'), may hold values from -0.3125 to 0.3125
- dense_mix: bfloat16 [1024], P('tp'), may hold values from -0.1875 to 0.1875
Outputs:
- layer_out: bfloat16 [128, 1024], P('ep', 'tp')
Inputs may be any that keep to these rules, and one draw needn't show every extreme that they name: `route_ids`: each row names 2 different experts. Among the 16 tokens of one index of ep no expert is named more than 8 times, and in every draw some expert is named exactly 8 times by the tokens of one index of ep.
All inputs are finite; a program needn't handle non-finite values.
Results may differ from a plain program's by a relative error of at most 0.013.
Values may be sent and summed in bfloat16 or wider, within the bound.
A program may use at most 64 MiB of HBM per device.

v0:
```python
import functools

import jax
import jax.numpy as jnp
from jax import lax
from jax.experimental import pallas as pl
from jax.experimental.pallas import tpu as pltpu
from jax.sharding import PartitionSpec as P

F32 = jnp.float32
BF16 = jnp.bfloat16
MESH = pl.DeviceIdType.MESH
EPS = 1e-06


def dot(a, b):
    return jnp.dot(a, b, preferred_element_type=F32)


def dot_t(a, b):
    return lax.dot_general(a, b, (((1,), (1,)), ((), ())), preferred_element_type=F32)


def column(row):
    n = row.shape[1]
    square = (n, n)
    eye = lax.broadcasted_iota(jnp.int32, square, 0) == lax.broadcasted_iota(jnp.int32, square, 1)
    return jnp.sum(jnp.where(eye, jnp.broadcast_to(row, square), 0.0), axis=1, keepdims=True)


def kernel(
    n_ep,
    n_tp,
    tokens,
    gain_mix,
    w_ig,
    w_fg,
    norm_state,
    max_state,
    gain_ffn,
    ids,
    logits,
    dense_mix,
    w_q,
    w_k,
    w_v,
    w_o,
    w_mix,
    cell,
    e_gate,
    e_up,
    e_down,
    d_gate,
    d_up,
    d_down,
    out,
    wp,
    wm,
    cs,
    eg,
    eu,
    ed,
    dg,
    du,
    dd,
    tok_all,
    mix_all,
    mix_own,
    dm_own,
    dm_all,
    rw_own,
    rw_all,
    res_own,
    res_all,
    xs,
    read,
    give,
    take,
    c_out,
    c_in,
    local_sem,
    send_sem,
    recv_sem,
    bulk_send,
    bulk_recv,
    word_sem,
):
    i = lax.axis_index("ep")
    j = lax.axis_index("tp")
    seq, quarter = tokens.shape
    head = cs.shape[-1]

    local = []

    def fetch(src, dst):
        copy = pltpu.make_async_copy(src, dst, local_sem.at[len(local)])
        copy.start()
        local.append(copy)
        return copy

    barrier = pltpu.get_barrier_semaphore()

    flips = [i + b - 2 * b * lax.rem(i // b, 2) for b in (1 << k for k in range(n_ep.bit_length() - 1))]
    hello = [(i, lax.rem(j + step, n_tp)) for step in range(1, n_tp)] + [(f, j) for f in flips]
    for peer in hello:
        pl.semaphore_signal(barrier, inc=1, device_id=peer, device_id_type=MESH)

    def tell(k):
        pl.semaphore_signal(word_sem.at[k], inc=1, device_id=(flips[k], j), device_id_type=MESH)

    def hear(k):
        pl.semaphore_wait(word_sem.at[k], 1)

    got_proj = [
        fetch(w, wp.at[:, pl.ds(k * head, head)]) for k, w in enumerate((w_q, w_k, w_v, w_o))
    ]
    got_cell = fetch(cell, cs)
    got_mix = fetch(w_mix, wm)
    got_eg = fetch(e_gate.at[0], eg)
    got_eu = fetch(e_up.at[0], eu)
    got_ed = fetch(e_down.at[0], ed)
    got_dg = fetch(d_gate, dg.at[j])
    got_du = fetch(d_up, du.at[j])
    got_dd = fetch(d_down, dd)

    l0, l1 = logits[0:1, :], logits[1:2, :]
    s0, s1 = jax.nn.sigmoid(l0 - l1), jax.nn.sigmoid(l1 - l0)

    def put_rw(e, carry):
        rw_own[e, :, 0:seq] = jnp.where(ids[0:1, :] == e, s0, 0.0) + jnp.where(
            ids[1:2, :] == e, s1, 0.0
        )
        return carry

    rw_own[...] = jnp.zeros_like(rw_own)
    lax.fori_loop(0, n_ep, put_rw, 0, unroll=8)
    rw_all[i] = rw_own[i]
    mix_row = dense_mix[...].astype(F32)
    mix_row = jnp.concatenate([mix_row[k : k + 1] for k in range(mix_row.shape[0])], axis=1)
    dm_own[...] = jnp.broadcast_to(mix_row, dm_own.shape)
    dm_all[j] = dm_own[...]
    tok_all[j] = tokens[...]

    pl.semaphore_wait(barrier, len(hello))
    tell(0)

    def to_tp(src, dst, phase):
        for step in range(1, n_tp):
            pltpu.make_async_remote_copy(
                src_ref=src,
                dst_ref=dst.at[j],
                send_sem=send_sem.at[phase],
                recv_sem=recv_sem.at[phase],
                device_id=(i, lax.rem(j + step, n_tp)),
                device_id_type=MESH,
            ).start()

    def wait_bytes(buf, count, sem):
        view = buf.at[pl.ds(0, count)]
        pltpu.make_async_copy(view, view, sem).wait()

    to_tp(tokens, tok_all, 0)

    near = j + 1 - 2 * lax.rem(j, 2)
    far = lax.rem(j + 2, n_tp)

    def bulk(src, buf, slot, peer, k):
        return pltpu.make_async_remote_copy(
            src_ref=src,
            dst_ref=buf.at[slot],
            send_sem=bulk_send.at[k],
            recv_sem=bulk_recv.at[k],
            device_id=(i, peer),
            device_id_type=MESH,
        )

    gate_far = bulk(d_gate, dg, j, far, 0)
    gate_near = bulk(d_gate, dg, j, near, 1)
    gate_on = bulk(dg.at[far], dg, far, near, 2)
    up_far = bulk(d_up, du, j, far, 3)
    up_near = bulk(d_up, du, j, near, 4)
    up_on = bulk(du.at[far], du, far, near, 5)
    gate_far.start()
    gate_near.start()
    up_near.start()

    def send_rw(step, carry):
        e = lax.rem(i + step, n_ep)
        pltpu.make_async_remote_copy(
            src_ref=rw_own.at[e],
            dst_ref=rw_all.at[i],
            send_sem=send_sem.at[1],
            recv_sem=recv_sem.at[1],
            device_id=(e, j),
            device_id_type=MESH,
        ).start()
        return carry

    to_tp(dm_own, dm_all, 2)

    wait_bytes(tok_all, n_tp - 1, recv_sem.at[0])
    hear(0)
    tell(1)
    full = jnp.concatenate([tok_all[k] for k in range(n_tp)], axis=1).astype(F32)
    scale = lax.rsqrt(jnp.mean(full * full, axis=-1, keepdims=True) + EPS)
    normed = (full * scale * gain_mix[...]).astype(BF16)
    normed_f = normed.astype(F32)
    ig = jnp.sum(normed_f * w_ig[...].astype(F32), axis=-1, keepdims=True)
    fg = jnp.sum(normed_f * w_fg[...].astype(F32), axis=-1, keepdims=True)
    for copy in got_proj:
        copy.wait()
    proj = dot(normed, wp[...])
    query = proj[:, :head]
    key = proj[:, head : 2 * head] * head ** (-0.5)
    value = proj[:, 2 * head : 3 * head]
    out_gate = proj[:, 3 * head :]
    carried = jnp.minimum(fg, 0.0) - jnp.log1p(jnp.exp(-jnp.abs(fg))) + column(max_state[...])
    stab = jnp.maximum(carried, ig)
    w_old = jnp.exp(carried - stab)
    w_new = jnp.exp(ig - stab) * jnp.sum(query * key, axis=-1, keepdims=True)
    got_cell.wait()
    query_t = query.T
    for b in range(seq):
        read[b : b + 1, :] = jnp.sum(query_t[:, b : b + 1] * cs[b], axis=0, keepdims=True)
    numer = w_old * read[...] + w_new * value
    denom = w_old * jnp.sum(query * norm_state[...], axis=-1, keepdims=True) + w_new
    cell_out = numer / jnp.maximum(jnp.abs(denom), 1.0)
    mixed = (jax.nn.sigmoid(out_gate) * cell_out).astype(BF16)
    mix_own[...] = mixed
    mix_all[j] = mixed
    to_tp(mix_own, mix_all, 3)
    for k in range(1, len(flips) - 1):
        hear(k)
        tell(k + 1)
    got_mix.wait()
    wait_bytes(mix_all, n_tp - 1, recv_sem.at[3])
    heads = jnp.concatenate([mix_all[k] for k in range(n_tp)], axis=1)
    resid = (tokens[...].astype(F32) + dot(heads, wm[...])).astype(BF16)
    res_own[...] = resid
    core = lax.rem(j, 2)
    half = n_tp // 2
    n_half = n_ep * half
    mine = i * half + j // 2
    res_all[core, mine] = resid

    def send_res(step, carry):
        peer = lax.rem(mine + step, n_half)
        pltpu.make_async_remote_copy(
            src_ref=res_own,
            dst_ref=res_all.at[core, mine],
            send_sem=send_sem.at[4],
            recv_sem=recv_sem.at[4],
            device_id=(peer // half, 2 * lax.rem(peer, half) + core),
            device_id_type=MESH,
        ).start()
        return carry

    hear(len(flips) - 1)
    lax.fori_loop(1, n_half, send_res, 0)
    lax.fori_loop(1, n_ep, send_rw, 0)
    up_far.start()
    gate_far.wait_recv()
    gate_on.start()

    wait_bytes(res_all.at[core], n_half - 1, recv_sem.at[4])
    res_on = pltpu.make_async_remote_copy(
        src_ref=res_all.at[core],
        dst_ref=res_all.at[core],
        send_sem=bulk_send.at[7],
        recv_sem=bulk_recv.at[7],
        device_id=(i, near),
        device_id_type=MESH,
    )
    res_on.start()

    wait_bytes(rw_all, n_ep - 1, recv_sem.at[1])
    wide = (n_ep, seq, rw_all.shape[-1])
    diag = lax.broadcasted_iota(jnp.int32, wide, 1) == lax.broadcasted_iota(jnp.int32, wide, 2)
    weight = jnp.where(diag, jnp.broadcast_to(rw_all[...], wide), 0.0)
    weight = jnp.sum(weight.reshape(n_ep * seq, -1), axis=-1, keepdims=True)
    wait_bytes(dm_all, n_tp - 1, recv_sem.at[2])

    res_on.wait_recv()
    rows = res_all[...].reshape(2, n_ep, half, seq, quarter)
    parts = [
        rows[k % 2, :, k // 2].reshape(n_ep * seq, quarter).astype(F32) for k in range(n_tp)
    ]
    square = sum(jnp.sum(p * p, axis=-1, keepdims=True) for p in parts)
    scale = lax.rsqrt(square / (n_tp * quarter) + EPS)
    logit = jnp.zeros_like(scale)
    for k in range(n_tp):
        cols = slice(k * quarter, (k + 1) * quarter)
        part = (parts[k] * scale * gain_ffn[:, cols]).astype(BF16)
        xs[:, cols] = part
        logit += jnp.sum(part.astype(F32) * dm_all[k][0:1, :], axis=-1, keepdims=True)
    mix_gate = jax.nn.sigmoid(logit)

    got_eg.wait()
    got_eu.wait()
    g = dot_t(xs[...], eg[...])
    u = dot_t(xs[...], eu[...])
    hidden = (g * jax.nn.sigmoid(g) * u).astype(BF16)
    up_far.wait_recv()
    up_on.start()
    got_ed.wait()
    def expert_part(tp_index):
        cols = pl.ds(pl.multiple_of(tp_index * quarter, quarter), quarter)
        return dot(hidden, ed[:, cols]) * weight

    for k in range(half):
        give[k] = expert_part(2 * k + 1 - core).astype(BF16).reshape(n_ep, seq, quarter)
    give_on = pltpu.make_async_remote_copy(
        src_ref=give,
        dst_ref=take,
        send_sem=bulk_send.at[6],
        recv_sem=bulk_recv.at[6],
        device_id=(i, near),
        device_id_type=MESH,
    )
    give_on.start()
    kept = [expert_part(2 * k + core) for k in range(half)]

    got_dg.wait()
    gate_near.wait_recv()
    gate_on.wait_recv()
    g = dot(xs[...], dg[...].reshape(n_tp * quarter, -1))
    got_du.wait()
    up_near.wait_recv()
    up_on.wait_recv()
    u = dot(xs[...], du[...].reshape(n_tp * quarter, -1))
    hidden = (g * jax.nn.sigmoid(g) * u).astype(BF16)
    got_dd.wait()
    dense = dot(hidden, dd[...]) * mix_gate
    give_on.wait_recv()
    for k in range(half):
        total = kept[k] + jnp.where(j // 2 == k, dense, 0.0)
        total += take[k].reshape(n_ep * seq, quarter).astype(F32)
        c_out[k] = total.astype(BF16).reshape(n_ep, seq, quarter)
    c_in[mine] = c_out[j // 2, i]

    def send_back(step, carry):
        peer = lax.rem(mine + step, n_half)
        pi, px = peer // half, lax.rem(peer, half)
        pltpu.make_async_remote_copy(
            src_ref=c_out.at[px, pi],
            dst_ref=c_in.at[mine],
            send_sem=send_sem.at[5],
            recv_sem=recv_sem.at[5],
            device_id=(pi, 2 * px + core),
            device_id_type=MESH,
        ).start()
        return carry

    lax.fori_loop(1, n_half, send_back, 0)

    wait_bytes(tok_all, n_tp - 1, send_sem.at[0])
    wait_bytes(rw_all, n_ep - 1, send_sem.at[1])
    wait_bytes(dm_all, n_tp - 1, send_sem.at[2])
    wait_bytes(mix_all, n_tp - 1, send_sem.at[3])
    wait_bytes(res_all.at[core], n_half - 1, send_sem.at[4])
    for copy in (gate_far, gate_near, gate_on, up_far, up_near, up_on, give_on, res_on):
        copy.wait_send()

    wait_bytes(c_in, n_half - 1, recv_sem.at[5])

    def add(k, total):
        return total + c_in[k].astype(F32)

    total = lax.fori_loop(0, n_half, add, res_own[...].astype(F32), unroll=8)
    out[...] = total.astype(BF16)
    wait_bytes(c_in, n_half - 1, send_sem.at[5])


def local(
    n_ep,
    n_tp,
    tokens,
    gain_mix,
    w_query,
    w_key,
    w_value,
    w_outgate,
    w_input_gate,
    w_forget_gate,
    w_mix_out,
    cell_state,
    norm_state,
    max_state,
    gain_ffn,
    route_ids,
    route_logits,
    expert_gate,
    expert_up,
    expert_down,
    dense_gate,
    dense_up,
    dense_down,
    dense_mix,
):
    seq, quarter = tokens.shape
    features, head = w_query.shape
    n_all = n_ep * n_tp
    ff = expert_gate.shape[2]
    dff = dense_gate.shape[1]
    vmem = pl.BlockSpec(memory_space=pltpu.VMEM)
    any_space = pl.BlockSpec(memory_space=pl.ANY)
    small = (
        tokens,
        gain_mix.reshape(1, -1),
        w_input_gate.reshape(1, -1),
        w_forget_gate.reshape(1, -1),
        norm_state.reshape(seq, head),
        max_state.T,
        gain_ffn.reshape(1, -1),
        route_ids.T,
        route_logits.T,
        dense_mix.reshape(-1, 128),
    )
    large = (
        w_query,
        w_key,
        w_value,
        w_outgate,
        w_mix_out,
        cell_state.reshape(seq, head, head),
        jnp.swapaxes(expert_gate, 1, 2),
        jnp.swapaxes(expert_up, 1, 2),
        expert_down,
        dense_gate,
        dense_up,
        dense_down,
    )
    return pl.pallas_call(
        functools.partial(kernel, n_ep, n_tp),
        out_shape=jax.ShapeDtypeStruct((seq, quarter), BF16),
        in_specs=[vmem] * len(small) + [any_space] * len(large),
        out_specs=vmem,
        scratch_shapes=[
            pltpu.VMEM((features, 4 * head), BF16),
            pltpu.VMEM(w_mix_out.shape, BF16),
            pltpu.VMEM((seq, head, head), F32),
            pltpu.VMEM((ff, features), BF16),
            pltpu.VMEM((ff, features), BF16),
            pltpu.VMEM((ff, features), BF16),
            pltpu.VMEM((n_tp, quarter, dff), BF16),
            pltpu.VMEM((n_tp, quarter, dff), BF16),
            pltpu.VMEM(dense_down.shape, BF16),
            pltpu.VMEM((n_tp, seq, quarter), BF16),
            pltpu.VMEM((n_tp, seq, head), BF16),
            pltpu.VMEM((seq, head), BF16),
            pltpu.VMEM((8, quarter), F32),
            pltpu.VMEM((n_tp, 8, quarter), F32),
            pltpu.VMEM((n_ep, 1, 128), F32),
            pltpu.VMEM((n_ep, 1, 128), F32),
            pltpu.VMEM((seq, quarter), BF16),
            pltpu.VMEM((2, n_all // 2, seq, quarter), BF16),
            pltpu.VMEM((n_ep * seq, features), BF16),
            pltpu.VMEM((seq, head), F32),
            pltpu.VMEM((n_tp // 2, n_ep, seq, quarter), BF16),
            pltpu.VMEM((n_tp // 2, n_ep, seq, quarter), BF16),
            pltpu.VMEM((n_tp // 2, n_ep, seq, quarter), BF16),
            pltpu.VMEM((n_all // 2, seq, quarter), BF16),
            pltpu.SemaphoreType.DMA((12,)),
            pltpu.SemaphoreType.DMA((6,)),
            pltpu.SemaphoreType.DMA((6,)),
            pltpu.SemaphoreType.DMA((8,)),
            pltpu.SemaphoreType.DMA((8,)),
            pltpu.SemaphoreType.REGULAR((n_ep.bit_length() - 1,)),
        ],
        compiler_params=pltpu.CompilerParams(
            collective_id=0, has_side_effects=True, vmem_limit_bytes=60 * 1024 * 1024
        ),
    )(*small, *large)


def solution(mesh):
    return jax.shard_map(
        functools.partial(local, mesh.shape["ep"], mesh.shape["tp"]),
        mesh=mesh,
        in_specs=(
            P("ep", "tp"),
            P(),
            P(None, "tp"),
            P(None, "tp"),
            P(None, "tp"),
            P(None, "tp"),
            P(None, "tp"),
            P(None, "tp"),
            P(None, "tp"),
            P("ep", "tp", None, None),
            P("ep", "tp", None),
            P("ep", "tp"),
            P(),
            P("ep", None),
            P("ep", None),
            P("ep", None, "tp"),
            P("ep", None, "tp"),
            P("ep", "tp", None),
            P("tp", "ep"),
            P("tp", "ep"),
            P("ep", "tp"),
            P("tp"),
        ),
        out_specs=P("ep", "tp"),
        check_vma=False,
    )
```

profile of v0, /device:TPU:0, one launch (start us, length us, event | category | flops | bytes accessed | tf_op | source)
XLA Modules:
  0.0 29.5 jit_solution(9410099042965938625)
XLA Ops:
  0.0 28.2 %shard_map.208 = bf16[16,256]{1,0:T(8,128)(2,1)} custom-call(bf16[16,256]{1,0:T(8,128)(2,1)} %tokens.1, f32[1,1024]{1,0:T(1,128)} %bitcast.16, bf16[1,1024]{1,0:T(2,128)(2,1)} %bitcast.17, bf16[1,1024]{1,0:T(2,128)(2,1)} %bitcast.18, f32[16,128]{1,0:T(8,128)} %bitcast.15, f32[1,16]{1,0:T(1,128)} %bitcast.22, f32[1,1024]{1,0:T(1,128)} %bitcast.19, ...), custom_call_target="tpu_custom_call" | custom-call | tf_op jit(solution)/shard_map/pallas_call | solution.py:433
  28.2 1.3 %copy.24 = bf16[16,256]{1,0:T(8,128)(2,1)} copy(bf16[16,256]{1,0:T(8,128)(2,1)} %shard_map.208) | data formatting | bytes 16384
where the time goes:
time: 29.7 us; the launch traced here: 29.5 us
  Pallas kernels  28.2 us (95%)
  local copies, waits for them, and re-layouts  1.3 us (4%)
    pallas_call x1, Pallas kernels, local(): pl.pallas_call(functools.partial(kernel, n_ep, n_tp), out_shape=jax.Shape...  28.2 us
    unnamed x1, local copies, waits for them, and re-layouts  1.3 us

commit v1 on v0

v1 whole, which is shorter than its diff:
```python
import functools

import jax
import jax.numpy as jnp
from jax import lax
from jax.experimental import pallas as pl
from jax.experimental.pallas import tpu as pltpu
from jax.sharding import PartitionSpec as P

F32 = jnp.float32
BF16 = jnp.bfloat16
MESH = pl.DeviceIdType.MESH
EPS = 1e-06


def dot(a, b):
    return jnp.dot(a, b, preferred_element_type=F32)


def dot_t(a, b):
    return lax.dot_general(a, b, (((1,), (1,)), ((), ())), preferred_element_type=F32)


def column(row):
    n = row.shape[1]
    square = (n, n)
    eye = lax.broadcasted_iota(jnp.int32, square, 0) == lax.broadcasted_iota(jnp.int32, square, 1)
    return jnp.sum(jnp.where(eye, jnp.broadcast_to(row, square), 0.0), axis=1, keepdims=True)


def kernel(
    n_ep,
    n_tp,
    tokens,
    gain_mix,
    w_ig,
    w_fg,
    norm_state,
    max_state,
    gain_ffn,
    ids,
    logits,
    dense_mix,
    w_q,
    w_k,
    w_v,
    w_o,
    w_mix,
    cell,
    e_gate,
    e_up,
    e_down,
    d_gate,
    d_up,
    d_down,
    out,
    tok,
    gm,
    ig_w,
    fg_w,
    ns,
    ms,
    gf,
    id_v,
    lg,
    dmx,
    wp,
    wm,
    cs,
    egu,
    ed,
    dg,
    du,
    dd,
    tok_all,
    mix_all,
    mix_own,
    dm_own,
    dm_all,
    rw_own,
    rw_all,
    res_own,
    res_all,
    read,
    give,
    take,
    c_out,
    c_in,
    local_sem,
    send_sem,
    recv_sem,
    bulk_send,
    bulk_recv,
    word_sem,
):
    i = lax.axis_index("ep")
    j = lax.axis_index("tp")
    seq, quarter = tok.shape
    head = cs.shape[-1]
    ff = e_gate.shape[1]
    lead = ff // 256 * 256
    tail = -(-(ff - lead) // 128) * 128
    half = n_tp // 2
    n_half = n_ep * half
    rows_all = n_ep * seq
    core = lax.rem(j, 2)
    other = 1 - core
    mine = i * half + j // 2
    near = j + 1 - 2 * core
    far = lax.rem(j + 2, n_tp)
    peers = [(i, lax.rem(j + step, n_tp)) for step in range(1, n_tp)]

    barrier = pltpu.get_barrier_semaphore()
    turns = [lax.rem(i + step, n_ep) for step in (n_ep // 4, n_ep - n_ep // 4)]
    bits = [1 << k for k in reversed(range(n_ep.bit_length() - 3))]
    flips = [i + b - 2 * b * lax.rem(i // b, 2) for b in bits]
    rounds = [[(t, j) for t in turns]] + [[(f, j)] for f in flips] + [peers]
    hello = peers + [p for r in rounds[:-1] for p in r]
    for peer in hello:
        pl.semaphore_signal(barrier, inc=1, device_id=peer, device_id_type=MESH)

    def tell(k):
        for peer in rounds[k]:
            pl.semaphore_signal(word_sem.at[k], inc=1, device_id=peer, device_id_type=MESH)

    def hear(k):
        pl.semaphore_wait(word_sem.at[k], len(rounds[k]))

    local = []

    def fetch(src, dst):
        copy = pltpu.make_async_copy(src, dst, local_sem.at[len(local)])
        copy.start()
        local.append(copy)
        return copy

    got_tok = fetch(tokens, tok)
    got_route = [fetch(ids, id_v), fetch(logits, lg), fetch(dense_mix, dmx)]
    got_norm = [fetch(gain_mix, gm), fetch(w_ig, ig_w), fetch(w_fg, fg_w)]
    got_proj = [
        fetch(w, wp.at[:, pl.ds(k * head, head)]) for k, w in enumerate((w_q, w_k, w_v, w_o))
    ]
    got_cell = [fetch(cell, cs), fetch(norm_state, ns), fetch(max_state, ms)]
    got_mix = fetch(w_mix, wm)
    got_gf = fetch(gain_ffn, gf)
    got_e = []
    for w, first, last in ((e_gate, 0, 2 * lead), (e_up, lead, 2 * lead + tail)):
        if lead:
            got_e.append(fetch(w.at[0, pl.ds(0, lead)], egu.at[pl.ds(first, lead)]))
        if ff > lead:
            rest = ff - lead
            got_e.append(fetch(w.at[0, pl.ds(lead, rest)], egu.at[pl.ds(last, rest)]))
    got_ed = fetch(e_down.at[0], ed)
    got_dg = fetch(d_gate, dg.at[j])
    got_du = fetch(d_up, du.at[j])

    def to_tp(src, dst, phase):
        for peer in peers:
            pltpu.make_async_remote_copy(
                src_ref=src,
                dst_ref=dst.at[j],
                send_sem=send_sem.at[phase],
                recv_sem=recv_sem.at[phase],
                device_id=peer,
                device_id_type=MESH,
            ).start()

    def wait_bytes(buf, count, sem):
        view = buf.at[pl.ds(0, count)]
        pltpu.make_async_copy(view, view, sem).wait()

    def bulk(src, dst, peer, k):
        return pltpu.make_async_remote_copy(
            src_ref=src,
            dst_ref=dst,
            send_sem=bulk_send.at[k],
            recv_sem=bulk_recv.at[k],
            device_id=(i, peer),
            device_id_type=MESH,
        )

    gate_far = bulk(d_gate, dg.at[j], far, 0)
    gate_near = bulk(d_gate, dg.at[j], near, 1)
    gate_on = bulk(dg.at[far], dg.at[far], near, 2)
    up_far = bulk(d_up, du.at[j], far, 3)
    up_near = bulk(d_up, du.at[j], near, 4)
    up_on = bulk(du.at[far], du.at[far], near, 5)
    give_on = bulk(give, take, near, 6)
    res_on = bulk(res_all.at[other], res_all.at[other], near, 7)
    down_near = bulk(d_down, dd, near, 8)

    got_tok.wait()
    pl.semaphore_wait(barrier, len(hello))
    to_tp(tok, tok_all, 0)
    tell(0)
    gate_near.start()
    up_near.start()
    down_near.start()
    gate_far.start()
    tok_all[j] = tok[...]
    for copy in got_route:
        copy.wait()
    l0, l1 = lg[0:1, :], lg[1:2, :]
    s0, s1 = jax.nn.sigmoid(l0 - l1), jax.nn.sigmoid(l1 - l0)

    def put_rw(e, carry):
        rw_own[e, :, 0:seq] = jnp.where(id_v[0:1, :] == e, s0, 0.0) + jnp.where(
            id_v[1:2, :] == e, s1, 0.0
        )
        return carry

    rw_own[...] = jnp.zeros_like(rw_own)
    lax.fori_loop(0, n_ep, put_rw, 0, unroll=8)
    rw_all[i] = rw_own[i]
    mix_row = dmx[...].astype(F32)
    mix_row = jnp.concatenate([mix_row[k : k + 1] for k in range(mix_row.shape[0])], axis=1)
    dm_own[...] = mix_row
    dm_all[j] = mix_row
    if tail > ff - lead > 0:
        for first in (2 * lead, 2 * lead + tail):
            blank = pl.ds(first + ff - lead, tail - ff + lead)
            egu[blank, :] = jnp.zeros((tail - ff + lead, egu.shape[1]), egu.dtype)
    for k in range(len(rounds) - 1):
        hear(k)
        tell(k + 1)
    to_tp(dm_own, dm_all, 2)

    def send_rw(step, carry):
        e = lax.rem(i + step, n_ep)
        pltpu.make_async_remote_copy(
            src_ref=rw_own.at[e],
            dst_ref=rw_all.at[i],
            send_sem=send_sem.at[1],
            recv_sem=recv_sem.at[1],
            device_id=(e, j),
            device_id_type=MESH,
        ).start()
        return carry

    lax.fori_loop(1, n_ep, send_rw, 0)

    for copy in got_norm:
        copy.wait()
    wait_bytes(tok_all, n_tp - 1, recv_sem.at[0])
    full = jnp.concatenate([tok_all[k] for k in range(n_tp)], axis=1).astype(F32)
    scale = lax.rsqrt(jnp.mean(full * full, axis=-1, keepdims=True) + EPS)
    normed = (full * scale * gm[...]).astype(BF16)
    normed_f = normed.astype(F32)
    ig = jnp.sum(normed_f * ig_w[...].astype(F32), axis=-1, keepdims=True)
    fg = jnp.sum(normed_f * fg_w[...].astype(F32), axis=-1, keepdims=True)
    for copy in got_proj:
        copy.wait()
    proj = dot(normed, wp[...])
    query = proj[:, :head]
    key = proj[:, head : 2 * head] * head ** (-0.5)
    value = proj[:, 2 * head : 3 * head]
    out_gate = proj[:, 3 * head :]
    for copy in got_cell:
        copy.wait()
    carried = jnp.minimum(fg, 0.0) - jnp.log1p(jnp.exp(-jnp.abs(fg))) + column(ms[...])
    stab = jnp.maximum(carried, ig)
    w_old = jnp.exp(carried - stab)
    w_new = jnp.exp(ig - stab) * jnp.sum(query * key, axis=-1, keepdims=True)
    query_t = query.T
    for b in range(seq):
        read[b : b + 1, :] = jnp.sum(query_t[:, b : b + 1] * cs[b], axis=0, keepdims=True)
    numer = w_old * read[...] + w_new * value
    denom = w_old * jnp.sum(query * ns[...], axis=-1, keepdims=True) + w_new
    cell_out = numer / jnp.maximum(jnp.abs(denom), 1.0)
    mixed = (jax.nn.sigmoid(out_gate) * cell_out).astype(BF16)
    mix_own[...] = mixed
    mix_all[j] = mixed
    to_tp(mix_own, mix_all, 3)
    up_far.start()
    hear(len(rounds) - 1)
    got_mix.wait()
    wait_bytes(mix_all, n_tp - 1, recv_sem.at[3])
    heads = jnp.concatenate([mix_all[k] for k in range(n_tp)], axis=1)
    resid = (tok[...].astype(F32) + dot(heads, wm[...])).astype(BF16)
    res_own[...] = resid

    ring = n_ep // 2

    def across(send):
        def body(t, carry):
            turn = (t + 1) // 2
            turn = lax.rem(ring // 2 + ring + jnp.where(lax.rem(t, 2) == 0, turn, -turn), ring)
            high = lax.rem(i // 2 + turn, ring)
            for low in (1, 0):
                row = 2 * high + lax.rem(i + low, 2)
                for step in reversed(range(half)):
                    send(row, lax.rem(j // 2 + step, half))
            return carry

        lax.fori_loop(0, ring, body, 0, unroll=ring <= 4)

    def send_res(row, col):
        pltpu.make_async_remote_copy(
            src_ref=res_own,
            dst_ref=res_all.at[core, mine],
            send_sem=send_sem.at[4],
            recv_sem=recv_sem.at[4],
            device_id=(row, 2 * col + other),
            device_id_type=MESH,
        ).start()
    across(send_res)
    gate_far.wait_recv()
    gate_on.start()
    wait_bytes(rw_all, n_ep - 1, recv_sem.at[1])
    wide = (n_ep, seq, rw_all.shape[-1])
    diag = lax.broadcasted_iota(jnp.int32, wide, 1) == lax.broadcasted_iota(jnp.int32, wide, 2)
    weight = jnp.where(diag, jnp.broadcast_to(rw_all[...], wide), 0.0)
    weight = jnp.sum(weight.reshape(rows_all, -1), axis=-1, keepdims=True)
    wait_bytes(dm_all, n_tp - 1, recv_sem.at[2])
    up_far.wait_recv()
    up_on.start()
    got_gf.wait()
    for copy in got_e:
        copy.wait()
    got_dg.wait()
    got_du.wait()
    gate_near.wait_recv()
    up_near.wait_recv()
    wait_bytes(res_all.at[other], n_half, recv_sem.at[4])
    res_on.start()

    def columns(part, k):
        return pl.ds(pl.multiple_of((2 * k + part) * quarter, quarter), quarter)

    def normalized(part):
        rows = res_all[part].reshape(n_ep, half, seq, quarter)
        cut, square, logit = [], 0.0, 0.0
        for k in range(half):
            block = rows[:, k].reshape(rows_all, quarter).astype(F32)
            square += jnp.sum(block * block, axis=-1, keepdims=True)
            block = (block * gf[:, columns(part, k)]).astype(BF16)
            logit += jnp.sum(block.astype(F32) * dm_all[2 * k + part], axis=-1, keepdims=True)
            cut.append(block)
        return cut, square, logit

    def expert_in(cut, part):
        return sum(dot_t(cut[k], egu[:, columns(part, k)]) for k in range(half))

    def dense_in(cut, part, w):
        return sum(dot(cut[k], w[2 * k + part]) for k in range(half))

    cut_a, square_a, logit_a = normalized(other)
    expert_a = expert_in(cut_a, other)
    gate_on.wait_recv()
    up_on.wait_recv()
    gate_a = dense_in(cut_a, other, dg)
    up_a = dense_in(cut_a, other, du)
    res_on.wait_recv()
    cut_b, square_b, logit_b = normalized(core)
    scale = lax.rsqrt((square_a + square_b) / (n_tp * quarter) + EPS)
    mix_gate = jax.nn.sigmoid((logit_a + logit_b) * scale)
    mids = (expert_a + expert_in(cut_b, core)) * scale

    def activated(g, u):
        return (g * jax.nn.sigmoid(g) * u).astype(BF16)

    rest = ff - lead
    hidden = []
    if lead:
        hidden.append(activated(mids[:, :lead], mids[:, lead : 2 * lead]))
    if rest:
        low = 2 * lead
        hidden.append(activated(mids[:, low : low + rest], mids[:, low + tail : low + tail + rest]))
    hidden = jnp.concatenate(hidden, axis=1)
    got_ed.wait()
    def expert_part(part, k):
        return dot(hidden, ed[:, columns(part, k)]) * weight

    for k in range(half):
        give[k] = expert_part(core, k).astype(BF16).reshape(n_ep, seq, quarter)
    give_on.start()
    kept = [expert_part(other, k) for k in range(half)]
    g = (gate_a + dense_in(cut_b, core, dg)) * scale
    u = (up_a + dense_in(cut_b, core, du)) * scale
    hidden = activated(g, u)
    down_near.wait_recv()
    dense = dot(hidden, dd[...]) * mix_gate
    give_on.wait_recv()
    for k in range(half):
        total = kept[k] + jnp.where(j // 2 == k, dense, 0.0)
        total += take[k].reshape(rows_all, quarter).astype(F32)
        c_out[k] = total.astype(BF16).reshape(n_ep, seq, quarter)

    def send_back(row, col):
        pltpu.make_async_remote_copy(
            src_ref=c_out.at[col, row],
            dst_ref=c_in.at[mine],
            send_sem=send_sem.at[5],
            recv_sem=recv_sem.at[5],
            device_id=(row, 2 * col + other),
            device_id_type=MESH,
        ).start()
    across(send_back)
    wait_bytes(tok_all, n_tp - 1, send_sem.at[0])
    wait_bytes(rw_all, n_ep - 1, send_sem.at[1])
    wait_bytes(dm_all, n_tp - 1, send_sem.at[2])
    wait_bytes(mix_all, n_tp - 1, send_sem.at[3])
    wait_bytes(res_all.at[other], n_half, send_sem.at[4])
    for copy in (gate_far, gate_near, gate_on, up_far, up_near, up_on, give_on, res_on, down_near):
        copy.wait_send()
    wait_bytes(c_in, n_half, send_sem.at[5])
    wait_bytes(c_in, n_half, recv_sem.at[5])
    def add(k, total):
        return total + c_in[k].astype(F32)

    total = lax.fori_loop(0, n_half, add, res_own[...].astype(F32), unroll=8)
    out[...] = total.astype(BF16)


def local(
    n_ep,
    n_tp,
    tokens,
    gain_mix,
    w_query,
    w_key,
    w_value,
    w_outgate,
    w_input_gate,
    w_forget_gate,
    w_mix_out,
    cell_state,
    norm_state,
    max_state,
    gain_ffn,
    route_ids,
    route_logits,
    expert_gate,
    expert_up,
    expert_down,
    dense_gate,
    dense_up,
    dense_down,
    dense_mix,
):
    seq, quarter = tokens.shape
    features, head = w_query.shape
    n_all = n_ep * n_tp
    ff = expert_gate.shape[2]
    dff = dense_gate.shape[1]
    vmem = pl.BlockSpec(memory_space=pltpu.VMEM)
    tail = -(-(ff % 256) // 128) * 128
    wide = 2 * (ff // 256 * 256 + tail)
    any_space = pl.BlockSpec(memory_space=pl.ANY)
    small = (
        tokens,
        gain_mix.reshape(1, -1),
        w_input_gate.reshape(1, -1),
        w_forget_gate.reshape(1, -1),
        norm_state.reshape(seq, head),
        max_state.T,
        gain_ffn.reshape(1, -1),
        route_ids.T,
        route_logits.T,
        dense_mix.reshape(-1, 128),
    )
    large = (
        w_query,
        w_key,
        w_value,
        w_outgate,
        w_mix_out,
        cell_state.reshape(seq, head, head),
        jnp.swapaxes(expert_gate, 1, 2),
        jnp.swapaxes(expert_up, 1, 2),
        expert_down,
        dense_gate,
        dense_up,
        dense_down,
    )
    return pl.pallas_call(
        functools.partial(kernel, n_ep, n_tp),
        out_shape=pltpu.VMEM((seq, quarter), BF16),
        in_specs=[any_space] * (len(small) + len(large)),
        out_specs=vmem,
        scratch_shapes=[pltpu.VMEM(x.shape, x.dtype) for x in small]
        + [
            pltpu.VMEM((features, 4 * head), BF16),
            pltpu.VMEM(w_mix_out.shape, BF16),
            pltpu.VMEM((seq, head, head), F32),
            pltpu.VMEM((wide, features), BF16),
            pltpu.VMEM((ff, features), BF16),
            pltpu.VMEM((n_tp, quarter, dff), BF16),
            pltpu.VMEM((n_tp, quarter, dff), BF16),
            pltpu.VMEM(dense_down.shape, BF16),
            pltpu.VMEM((n_tp, seq, quarter), BF16),
            pltpu.VMEM((n_tp, seq, head), BF16),
            pltpu.VMEM((seq, head), BF16),
            pltpu.VMEM((1, quarter), F32),
            pltpu.VMEM((n_tp, 1, quarter), F32),
            pltpu.VMEM((n_ep, 1, 128), F32),
            pltpu.VMEM((n_ep, 1, 128), F32),
            pltpu.VMEM((seq, quarter), BF16),
            pltpu.VMEM((2, n_all // 2, seq, quarter), BF16),
            pltpu.VMEM((seq, head), F32),
            pltpu.VMEM((n_tp // 2, n_ep, seq, quarter), BF16),
            pltpu.VMEM((n_tp // 2, n_ep, seq, quarter), BF16),
            pltpu.VMEM((n_tp // 2, n_ep, seq, quarter), BF16),
            pltpu.VMEM((n_all // 2, seq, quarter), BF16),
            pltpu.SemaphoreType.DMA((24,)),
            pltpu.SemaphoreType.DMA((6,)),
            pltpu.SemaphoreType.DMA((6,)),
            pltpu.SemaphoreType.DMA((9,)),
            pltpu.SemaphoreType.DMA((9,)),
            pltpu.SemaphoreType.REGULAR((n_ep.bit_length() - 1,)),
        ],
        compiler_params=pltpu.CompilerParams(
            collective_id=0, has_side_effects=True, vmem_limit_bytes=60 * 1024 * 1024
        ),
    )(*small, *large)


def solution(mesh):
    return jax.shard_map(
        functools.partial(local, mesh.shape["ep"], mesh.shape["tp"]),
        mesh=mesh,
        in_specs=(
            P("ep", "tp"),
            P(),
            P(None, "tp"),
            P(None, "tp"),
            P(None, "tp"),
            P(None, "tp"),
            P(None, "tp"),
            P(None, "tp"),
            P(None, "tp"),
            P("ep", "tp", None, None),
            P("ep", "tp", None),
            P("ep", "tp"),
            P(),
            P("ep", None),
            P("ep", None),
            P("ep", None, "tp"),
            P("ep", None, "tp"),
            P("ep", "tp", None),
            P("tp", "ep"),
            P("tp", "ep"),
            P("ep", "tp"),
            P("tp"),
        ),
        out_specs=P("ep", "tp"),
        check_vma=False,
    )
```

time: 29.7 us -> 27.3 us (0.919)
  Pallas kernels: 28.2 us -> 26.5 us
  local copies, waits for them, and re-layouts: 1.3 us -> 0.6 us
    pallas_call x1, Pallas kernels: 28.2 us -> 26.5 us  [local(): pl.pallas_call(functools.partial(kernel, n_ep, n_tp), out_shape=pltpu.VME...]
    unnamed x1, local copies, waits for them, and re-layouts: 1.3 us -> 0.6 us
where the time goes in v1:
time: 27.3 us; the launch traced here: 27.1 us
  Pallas kernels  26.5 us (97%)
  local copies, waits for them, and re-layouts  0.6 us (2%)
    pallas_call x1, Pallas kernels, local(): pl.pallas_call(functools.partial(kernel, n_ep, n_tp), out_shape=pltpu.VME...  26.5 us
    unnamed x1, local copies, waits for them, and re-layouts  0.6 us

profile of v1, /device:TPU:0, one launch (start us, length us, event | category | flops | bytes accessed | tf_op | source)
XLA Modules:
  0.0 27.1 jit_solution(18132273634696607994)
XLA Ops:
  0.0 26.5 %shard_map.208 = bf16[16,256]{1,0:T(8,128)(2,1)S(1)} custom-call(bf16[16,256]{1,0:T(8,128)(2,1)} %tokens.1, f32[1,1024]{1,0:T(1,128)} %bitcast.16, bf16[1,1024]{1,0:T(2,128)(2,1)} %bitcast.17, bf16[1,1024]{1,0:T(2,128)(2,1)} %bitcast.18, f32[16,128]{1,0:T(8,128)} %bitcast.15, f32[1,16]{1,0:T(1,128)} %bitcast.22, f32[1,1024]{1,0:T(1,128)} %bitcast.19, ...), custom_call_target="tpu_custom_call" | custom-call | tf_op jit(solution)/shard_map/pallas_call | solution.py:476
  26.5 0.6 %copy.24 = bf16[16,256]{1,0:T(8,128)(2,1)} copy(bf16[16,256]{1,0:T(8,128)(2,1)S(1)} %shard_map.208) | data formatting | bytes 16384

commit v2 on v1

--- a/solution.py
+++ b/solution.py
@@ -72,6 +72,11 @@
     dg,
     du,
     dd,
+    dgu,
+    pack,
+    down_own,
+    down_far,
+    down,
     tok_all,
     mix_all,
     mix_own,
@@ -110,21 +115,36 @@
     far = lax.rem(j + 2, n_tp)
     peers = [(i, lax.rem(j + step, n_tp)) for step in range(1, n_tp)]
 
+    cross = lax.rem(near + 2, n_tp)
+    span = n_ep // 4
+    place = i // span
+    group = place // 2
+
     barrier = pltpu.get_barrier_semaphore()
-    turns = [lax.rem(i + step, n_ep) for step in (n_ep // 4, n_ep - n_ep // 4)]
     bits = [1 << k for k in reversed(range(n_ep.bit_length() - 3))]
     flips = [i + b - 2 * b * lax.rem(i // b, 2) for b in bits]
-    rounds = [[(t, j) for t in turns]] + [[(f, j)] for f in flips] + [peers]
-    hello = peers + [p for r in rounds[:-1] for p in r]
-    for peer in hello:
-        pl.semaphore_signal(barrier, inc=1, device_id=peer, device_id_type=MESH)
-
-    def tell(k):
-        for peer in rounds[k]:
-            pl.semaphore_signal(word_sem.at[k], inc=1, device_id=peer, device_id_type=MESH)
-
-    def hear(k):
-        pl.semaphore_wait(word_sem.at[k], len(rounds[k]))
+    lines = jnp.where(place > 0, 1, 0) + jnp.where(place < 3, 1, 0)
+
+    def signal(sem, peer):
+        pl.semaphore_signal(sem, inc=1, device_id=peer, device_id_type=MESH)
+
+    def along_line(sem):
+        @pl.when(place > 0)
+        def _():
+            signal(sem, (i - span, j))
+
+        @pl.when(place < 3)
+        def _():
+            signal(sem, (i + span, j))
+
+    for peer in peers:
+        signal(barrier, peer)
+
+    @pl.when(core == 1)
+    def _():
+        along_line(barrier)
+        for f in flips:
+            signal(barrier, (f, j))
 
     local = []
 
@@ -136,6 +156,7 @@
 
     got_tok = fetch(tokens, tok)
     got_route = [fetch(ids, id_v), fetch(logits, lg), fetch(dense_mix, dmx)]
+    got_dense = [fetch(d_gate, dg), fetch(d_up, du)]
     got_norm = [fetch(gain_mix, gm), fetch(w_ig, ig_w), fetch(w_fg, fg_w)]
     got_proj = [
         fetch(w, wp.at[:, pl.ds(k * head, head)]) for k, w in enumerate((w_q, w_k, w_v, w_o))
@@ -151,8 +172,7 @@
             rest = ff - lead
             got_e.append(fetch(w.at[0, pl.ds(lead, rest)], egu.at[pl.ds(last, rest)]))
     got_ed = fetch(e_down.at[0], ed)
-    got_dg = fetch(d_gate, dg.at[j])
-    got_du = fetch(d_up, du.at[j])
+    got_dd = fetch(d_down, dd)
 
     def to_tp(src, dst, phase):
         for peer in peers:
@@ -179,24 +199,27 @@
             device_id_type=MESH,
         )
 
-    gate_far = bulk(d_gate, dg.at[j], far, 0)
-    gate_near = bulk(d_gate, dg.at[j], near, 1)
-    gate_on = bulk(dg.at[far], dg.at[far], near, 2)
-    up_far = bulk(d_up, du.at[j], far, 3)
-    up_near = bulk(d_up, du.at[j], near, 4)
-    up_on = bulk(du.at[far], du.at[far], near, 5)
-    give_on = bulk(give, take, near, 6)
-    res_on = bulk(res_all.at[other], res_all.at[other], near, 7)
-    down_near = bulk(d_down, dd, near, 8)
+    top, low = pl.ds(0, quarter // 2), pl.ds(quarter // 2, quarter // 2)
+    far_top = bulk(pack.at[top], dgu.at[j, top], far, 0)
+    far_low = bulk(pack.at[low], dgu.at[j, low], far, 1)
+    near_gu = bulk(dgu.at[j], dgu.at[j], near, 2)
+    near_on = bulk(dgu.at[far], dgu.at[far], near, 3)
+    near_down = bulk(down_own, down.at[j // 2], near, 4)
+    cross_down = bulk(down_far, down.at[j // 2], cross, 5)
+    give_on = [bulk(give.at[g], take.at[g], near, 6 + g) for g in range(2)]
+    blocks = [pl.ds(g * (n_half // 2), n_half // 2) for g in range(2)]
+    res_on = [
+        bulk(res_all.at[other, b], res_all.at[other, b], near, 8 + g) for g, b in enumerate(blocks)
+    ]
 
     got_tok.wait()
-    pl.semaphore_wait(barrier, len(hello))
+    pl.semaphore_wait(barrier, len(peers) + core * (lines + len(flips)))
     to_tp(tok, tok_all, 0)
-    tell(0)
-    gate_near.start()
-    up_near.start()
-    down_near.start()
-    gate_far.start()
+
+    @pl.when(core == 1)
+    def _():
+        along_line(word_sem.at[0])
+
     tok_all[j] = tok[...]
     for copy in got_route:
         copy.wait()
@@ -220,25 +243,28 @@
         for first in (2 * lead, 2 * lead + tail):
             blank = pl.ds(first + ff - lead, tail - ff + lead)
             egu[blank, :] = jnp.zeros((tail - ff + lead, egu.shape[1]), egu.dtype)
-    for k in range(len(rounds) - 1):
-        hear(k)
-        tell(k + 1)
+
     to_tp(dm_own, dm_all, 2)
-
-    def send_rw(step, carry):
-        e = lax.rem(i + step, n_ep)
-        pltpu.make_async_remote_copy(
-            src_ref=rw_own.at[e],
-            dst_ref=rw_all.at[i],
-            send_sem=send_sem.at[1],
-            recv_sem=recv_sem.at[1],
-            device_id=(e, j),
-            device_id_type=MESH,
-        ).start()
-        return carry
-
-    lax.fori_loop(1, n_ep, send_rw, 0)
-
+    for copy in got_dense:
+        copy.wait()
+    dff = dg.shape[1]
+    mid = dff // 2
+    square = (dff, dff)
+    from_row = lax.broadcasted_iota(jnp.int32, square, 0)
+    to_col = lax.broadcasted_iota(jnp.int32, square, 1)
+
+    def pick(hit):
+        return jnp.where(hit, 1.0, 0.0).astype(BF16)
+
+    def packed(part):
+        first = pick((from_row == to_col + part * mid) & (to_col < mid))
+        second = pick((from_row == to_col - mid + part * mid) & (to_col >= mid))
+        return (dot(dg[...], first) + dot(du[...], second)).astype(BF16)
+
+    pack[...] = packed(1 - j // 2)
+    dgu[j] = packed(j // 2)
+    far_top.start()
+    near_gu.start()
     for copy in got_norm:
         copy.wait()
     wait_bytes(tok_all, n_tp - 1, recv_sem.at[0])
@@ -248,6 +274,11 @@
     normed_f = normed.astype(F32)
     ig = jnp.sum(normed_f * ig_w[...].astype(F32), axis=-1, keepdims=True)
     fg = jnp.sum(normed_f * fg_w[...].astype(F32), axis=-1, keepdims=True)
+
+    @pl.when(core == 1)
+    def _():
+        pl.semaphore_wait(word_sem.at[0], lines)
+        signal(word_sem.at[1], (i + 2 * span - 4 * span * group, j))
     for copy in got_proj:
         copy.wait()
     proj = dot(normed, wp[...])
@@ -271,8 +302,28 @@
     mix_own[...] = mixed
     mix_all[j] = mixed
     to_tp(mix_own, mix_all, 3)
-    up_far.start()
-    hear(len(rounds) - 1)
+    far_low.start()
+
+    @pl.when(core == 1)
+    def _():
+        pl.semaphore_wait(word_sem.at[1], 1)
+        for k, f in enumerate(flips):
+            signal(word_sem.at[2 + k], (f, j))
+            pl.semaphore_wait(word_sem.at[2 + k], 1)
+        signal(word_sem.at[2 + len(flips)], (i, near))
+    got_dd.wait()
+    some = (down_own.shape[0], dff)
+    to_row = lax.broadcasted_iota(jnp.int32, some, 0)
+    from_row = lax.broadcasted_iota(jnp.int32, some, 1)
+
+    def half_rows(part):
+        hit = (from_row == to_row + part * mid) & (to_row < mid)
+        return dot(pick(hit), dd[...]).astype(BF16)
+
+    down_own[...] = half_rows(j // 2)
+    down_far[...] = half_rows(1 - j // 2)
+    near_down.start()
+
     got_mix.wait()
     wait_bytes(mix_all, n_tp - 1, recv_sem.at[3])
     heads = jnp.concatenate([mix_all[k] for k in range(n_tp)], axis=1)
@@ -286,8 +337,8 @@
             turn = (t + 1) // 2
             turn = lax.rem(ring // 2 + ring + jnp.where(lax.rem(t, 2) == 0, turn, -turn), ring)
             high = lax.rem(i // 2 + turn, ring)
-            for low in (1, 0):
-                row = 2 * high + lax.rem(i + low, 2)
+            for down_y in (1, 0):
+                row = 2 * high + lax.rem(i + down_y, 2)
                 for step in reversed(range(half)):
                     send(row, lax.rem(j // 2 + step, half))
             return carry
@@ -299,109 +350,143 @@
             src_ref=res_own,
             dst_ref=res_all.at[core, mine],
             send_sem=send_sem.at[4],
-            recv_sem=recv_sem.at[4],
+            recv_sem=recv_sem.at[4 + 2 * group],
             device_id=(row, 2 * col + other),
             device_id_type=MESH,
         ).start()
+
+    @pl.when(core == 0)
+    def _():
+        pl.semaphore_wait(word_sem.at[2 + len(flips)], 1)
+
+    def send_rw(step, carry):
+        e = lax.rem(i + step, n_ep)
+        pltpu.make_async_remote_copy(
+            src_ref=rw_own.at[e],
+            dst_ref=rw_all.at[i],
+            send_sem=send_sem.at[1],
+            recv_sem=recv_sem.at[1 + 6 * group],
+            device_id=(e, j),
+            device_id_type=MESH,
+        ).start()
+        return carry
+
+    lax.fori_loop(1, n_ep, send_rw, 0)
+
     across(send_res)
-    gate_far.wait_recv()
-    gate_on.start()
-    wait_bytes(rw_all, n_ep - 1, recv_sem.at[1])
-    wide = (n_ep, seq, rw_all.shape[-1])
-    diag = lax.broadcasted_iota(jnp.int32, wide, 1) == lax.broadcasted_iota(jnp.int32, wide, 2)
-    weight = jnp.where(diag, jnp.broadcast_to(rw_all[...], wide), 0.0)
-    weight = jnp.sum(weight.reshape(rows_all, -1), axis=-1, keepdims=True)
+    far_top.wait_recv()
+    far_low.wait_recv()
+    near_on.start()
+    cross_down.start()
     wait_bytes(dm_all, n_tp - 1, recv_sem.at[2])
-    up_far.wait_recv()
-    up_on.start()
     got_gf.wait()
     for copy in got_e:
         copy.wait()
-    got_dg.wait()
-    got_du.wait()
-    gate_near.wait_recv()
-    up_near.wait_recv()
-    wait_bytes(res_all.at[other], n_half, recv_sem.at[4])
-    res_on.start()
+    near_gu.wait_recv()
+    got_ed.wait()
+
+    lot = rows_all // 2
 
     def columns(part, k):
         return pl.ds(pl.multiple_of((2 * k + part) * quarter, quarter), quarter)
 
-    def normalized(part):
-        rows = res_all[part].reshape(n_ep, half, seq, quarter)
-        cut, square, logit = [], 0.0, 0.0
-        for k in range(half):
-            block = rows[:, k].reshape(rows_all, quarter).astype(F32)
-            square += jnp.sum(block * block, axis=-1, keepdims=True)
-            block = (block * gf[:, columns(part, k)]).astype(BF16)
-            logit += jnp.sum(block.astype(F32) * dm_all[2 * k + part], axis=-1, keepdims=True)
-            cut.append(block)
-        return cut, square, logit
-
-    def expert_in(cut, part):
-        return sum(dot_t(cut[k], egu[:, columns(part, k)]) for k in range(half))
-
-    def dense_in(cut, part, w):
-        return sum(dot(cut[k], w[2 * k + part]) for k in range(half))
-
-    cut_a, square_a, logit_a = normalized(other)
-    expert_a = expert_in(cut_a, other)
-    gate_on.wait_recv()
-    up_on.wait_recv()
-    gate_a = dense_in(cut_a, other, dg)
-    up_a = dense_in(cut_a, other, du)
-    res_on.wait_recv()
-    cut_b, square_b, logit_b = normalized(core)
-    scale = lax.rsqrt((square_a + square_b) / (n_tp * quarter) + EPS)
-    mix_gate = jax.nn.sigmoid((logit_a + logit_b) * scale)
-    mids = (expert_a + expert_in(cut_b, core)) * scale
-
     def activated(g, u):
         return (g * jax.nn.sigmoid(g) * u).astype(BF16)
 
-    rest = ff - lead
-    hidden = []
-    if lead:
-        hidden.append(activated(mids[:, :lead], mids[:, lead : 2 * lead]))
-    if rest:
-        low = 2 * lead
-        hidden.append(activated(mids[:, low : low + rest], mids[:, low + tail : low + tail + rest]))
-    hidden = jnp.concatenate(hidden, axis=1)
-    got_ed.wait()
-    def expert_part(part, k):
-        return dot(hidden, ed[:, columns(part, k)]) * weight
-
-    for k in range(half):
-        give[k] = expert_part(core, k).astype(BF16).reshape(n_ep, seq, quarter)
-    give_on.start()
-    kept = [expert_part(other, k) for k in range(half)]
-    g = (gate_a + dense_in(cut_b, core, dg)) * scale
-    u = (up_a + dense_in(cut_b, core, du)) * scale
-    hidden = activated(g, u)
-    down_near.wait_recv()
-    dense = dot(hidden, dd[...]) * mix_gate
-    give_on.wait_recv()
-    for k in range(half):
-        total = kept[k] + jnp.where(j // 2 == k, dense, 0.0)
-        total += take[k].reshape(rows_all, quarter).astype(F32)
-        c_out[k] = total.astype(BF16).reshape(n_ep, seq, quarter)
-
-    def send_back(row, col):
-        pltpu.make_async_remote_copy(
-            src_ref=c_out.at[col, row],
-            dst_ref=c_in.at[mine],
-            send_sem=send_sem.at[5],
-            recv_sem=recv_sem.at[5],
-            device_id=(row, 2 * col + other),
-            device_id_type=MESH,
-        ).start()
-    across(send_back)
+    for g in range(2):
+        def normalized(part):
+            rows = res_all[part, blocks[g]].reshape(n_ep // 2, half, seq, quarter)
+            cut, square, logit = [], 0.0, 0.0
+            for k in range(half):
+                block = rows[:, k].reshape(lot, quarter).astype(F32)
+                square += jnp.sum(block * block, axis=-1, keepdims=True)
+                block = (block * gf[:, columns(part, k)]).astype(BF16)
+                logit += jnp.sum(block.astype(F32) * dm_all[2 * k + part], axis=-1, keepdims=True)
+                cut.append(block)
+            return cut, square, logit
+
+        def expert_in(cut, part):
+            return sum(dot_t(cut[k], egu[:, columns(part, k)]) for k in range(half))
+
+        def dense_in(cut, part):
+            return sum(dot(cut[k], dgu[2 * k + part]) for k in range(half))
+        wait_bytes(res_all.at[other], n_half // 2, recv_sem.at[4 + 2 * g])
+        res_on[g].start()
+        cut_a, square_a, logit_a = normalized(other)
+        expert_a = expert_in(cut_a, other)
+        if g == 0:
+            near_on.wait_recv()
+        dense_a = dense_in(cut_a, other)
+        res_on[g].wait_recv()
+        cut_b, square_b, logit_b = normalized(core)
+        scale = lax.rsqrt((square_a + square_b) / (n_tp * quarter) + EPS)
+        mix_gate = jax.nn.sigmoid((logit_a + logit_b) * scale)
+        mids = (expert_a + expert_in(cut_b, core)) * scale
+        rest = ff - lead
+        hidden = []
+        if lead:
+            hidden.append(activated(mids[:, :lead], mids[:, lead : 2 * lead]))
+        if rest:
+            at = 2 * lead
+            hidden.append(activated(mids[:, at : at + rest], mids[:, at + tail : at + tail + rest]))
+        hidden = jnp.concatenate(hidden, axis=1)
+        for here in range(2):
+
+            @pl.when(group == here)
+            def _():
+                wait_bytes(rw_all, n_ep // 2 - (here == g), recv_sem.at[1 + 6 * g])
+
+        wide = (n_ep // 2, seq, rw_all.shape[-1])
+        to_lane = lax.broadcasted_iota(jnp.int32, wide, 2)
+        diag = lax.broadcasted_iota(jnp.int32, wide, 1) == to_lane
+        mine_rw = rw_all[pl.ds(g * (n_ep // 2), n_ep // 2)]
+        some = jnp.where(diag, jnp.broadcast_to(mine_rw, wide), 0.0)
+        some = jnp.sum(some.reshape(lot, -1), axis=-1, keepdims=True)
+        def expert_part(part, k):
+            return dot(hidden, ed[:, columns(part, k)]) * some
+
+        for k in range(half):
+            give[g, k] = expert_part(core, k).astype(BF16).reshape(n_ep // 2, seq, quarter)
+        give_on[g].start()
+        kept = [expert_part(other, k) for k in range(half)]
+        mids = (dense_a + dense_in(cut_b, core)) * scale
+        middle = activated(mids[:, :mid], mids[:, mid : 2 * mid])
+        if g == 0:
+            near_down.wait_recv()
+            cross_down.wait_recv()
+        for k in range(half):
+            kept[k] += dot(middle, down[k, 0:mid]) * mix_gate
+        give_on[g].wait_recv()
+        for k in range(half):
+            total = kept[k] + take[g, k].reshape(lot, quarter).astype(F32)
+            c_out[k, pl.ds(g * (n_ep // 2), n_ep // 2)] = total.astype(BF16).reshape(
+                n_ep // 2, seq, quarter
+            )
+        first = jnp.where(group == g, 1, 0)
+
+        def send_back(t, carry):
+            high = g * (ring // 2) + lax.rem(i // 2 + first + t, ring // 2)
+            for down_y in (1, 0):
+                row = 2 * high + lax.rem(i + down_y, 2)
+                for step in reversed(range(half)):
+                    col = lax.rem(j // 2 + step, half)
+                    pltpu.make_async_remote_copy(
+                        src_ref=c_out.at[col, row],
+                        dst_ref=c_in.at[mine],
+                        send_sem=send_sem.at[5],
+                        recv_sem=recv_sem.at[5],
+                        device_id=(row, 2 * col + other),
+                        device_id_type=MESH,
+                    ).start()
+            return carry
+
+        lax.fori_loop(0, ring // 2, send_back, 0, unroll=ring <= 4)
     wait_bytes(tok_all, n_tp - 1, send_sem.at[0])
     wait_bytes(rw_all, n_ep - 1, send_sem.at[1])
     wait_bytes(dm_all, n_tp - 1, send_sem.at[2])
     wait_bytes(mix_all, n_tp - 1, send_sem.at[3])
     wait_bytes(res_all.at[other], n_half, send_sem.at[4])
-    for copy in (gate_far, gate_near, gate_on, up_far, up_near, up_on, give_on, res_on, down_near):
+    for copy in [far_top, far_low, near_gu, near_on, near_down, cross_down] + give_on + res_on:
         copy.wait_send()
     wait_bytes(c_in, n_half, send_sem.at[5])
     wait_bytes(c_in, n_half, recv_sem.at[5])
@@ -443,6 +528,7 @@
     n_all = n_ep * n_tp
     ff = expert_gate.shape[2]
     dff = dense_gate.shape[1]
+    dff_rows = -(-dff // 32) * 16
     vmem = pl.BlockSpec(memory_space=pltpu.VMEM)
     tail = -(-(ff % 256) // 128) * 128
     wide = 2 * (ff // 256 * 256 + tail)
@@ -485,9 +571,14 @@
             pltpu.VMEM((seq, head, head), F32),
             pltpu.VMEM((wide, features), BF16),
             pltpu.VMEM((ff, features), BF16),
+            pltpu.VMEM((quarter, dff), BF16),
+            pltpu.VMEM((quarter, dff), BF16),
+            pltpu.VMEM((dff, quarter), BF16),
             pltpu.VMEM((n_tp, quarter, dff), BF16),
-            pltpu.VMEM((n_tp, quarter, dff), BF16),
-            pltpu.VMEM(dense_down.shape, BF16),
+            pltpu.VMEM((quarter, dff), BF16),
+            pltpu.VMEM((dff_rows, quarter), BF16),
+            pltpu.VMEM((dff_rows, quarter), BF16),
+            pltpu.VMEM((n_tp // 2, dff_rows, quarter), BF16),
             pltpu.VMEM((n_tp, seq, quarter), BF16),
             pltpu.VMEM((n_tp, seq, head), BF16),
             pltpu.VMEM((seq, head), BF16),
@@ -498,16 +589,16 @@
             pltpu.VMEM((seq, quarter), BF16),
             pltpu.VMEM((2, n_all // 2, seq, quarter), BF16),
             pltpu.VMEM((seq, head), F32),
-            pltpu.VMEM((n_tp // 2, n_ep, seq, quarter), BF16),
-            pltpu.VMEM((n_tp // 2, n_ep, seq, quarter), BF16),
+            pltpu.VMEM((2, n_tp // 2, n_ep // 2, seq, quarter), BF16),
+            pltpu.VMEM((2, n_tp // 2, n_ep // 2, seq, quarter), BF16),
             pltpu.VMEM((n_tp // 2, n_ep, seq, quarter), BF16),
             pltpu.VMEM((n_all // 2, seq, quarter), BF16),
             pltpu.SemaphoreType.DMA((24,)),
-            pltpu.SemaphoreType.DMA((6,)),
-            pltpu.SemaphoreType.DMA((6,)),
-            pltpu.SemaphoreType.DMA((9,)),
-            pltpu.SemaphoreType.DMA((9,)),
-            pltpu.SemaphoreType.REGULAR((n_ep.bit_length() - 1,)),
+            pltpu.SemaphoreType.DMA((8,)),
+            pltpu.SemaphoreType.DMA((8,)),
+            pltpu.SemaphoreType.DMA((10,)),
+            pltpu.SemaphoreType.DMA((10,)),
+            pltpu.SemaphoreType.REGULAR((n_ep.bit_length(),)),
         ],
         compiler_params=pltpu.CompilerParams(
             collective_id=0, has_side_effects=True, vmem_limit_bytes=60 * 1024 * 1024

time: 27.3 us -> 24.4 us (0.89)
  Pallas kernels: 26.5 us -> 23.6 us
    pallas_call x1, Pallas kernels: 26.5 us -> 23.6 us  [local(): pl.pallas_call(functools.partial(kernel, n_ep, n_tp), out_shape=pltpu.VME...]
where the time goes in v2:
time: 24.4 us; the launch traced here: 24.2 us
  Pallas kernels  23.6 us (97%)
  local copies, waits for them, and re-layouts  0.6 us (2%)
    pallas_call x1, Pallas kernels, local(): pl.pallas_call(functools.partial(kernel, n_ep, n_tp), out_shape=pltpu.VME...  23.6 us
    unnamed x1, local copies, waits for them, and re-layouts  0.6 us

profile of v2, /device:TPU:0, one launch (start us, length us, event | category | flops | bytes accessed | tf_op | source)
XLA Modules:
  0.0 24.2 jit_solution(3813591174761728228)
XLA Ops:
  0.0 23.6 %shard_map.208 = bf16[16,256]{1,0:T(8,128)(2,1)S(1)} custom-call(bf16[16,256]{1,0:T(8,128)(2,1)} %tokens.1, f32[1,1024]{1,0:T(1,128)} %bitcast.16, bf16[1,1024]{1,0:T(2,128)(2,1)} %bitcast.17, bf16[1,1024]{1,0:T(2,128)(2,1)} %bitcast.18, f32[16,128]{1,0:T(8,128)} %bitcast.15, f32[1,16]{1,0:T(1,128)} %bitcast.22, f32[1,1024]{1,0:T(1,128)} %bitcast.19, ...), custom_call_target="tpu_custom_call" | custom-call | tf_op jit(solution)/shard_map/pallas_call | solution.py:562
  23.6 0.6 %copy.24 = bf16[16,256]{1,0:T(8,128)(2,1)} copy(bf16[16,256]{1,0:T(8,128)(2,1)S(1)} %shard_map.208) | data formatting | bytes 16384

commit v3 on v2

--- a/solution.py
+++ b/solution.py
@@ -9,6 +9,7 @@
 
 F32 = jnp.float32
 BF16 = jnp.bfloat16
+N_LOCAL = 6
 MESH = pl.DeviceIdType.MESH
 EPS = 1e-06
 
@@ -68,6 +69,7 @@
     wm,
     cs,
     egu,
+    turned,
     ed,
     dg,
     du,
@@ -146,33 +148,29 @@
         for f in flips:
             signal(barrier, (f, j))
 
-    local = []
-
-    def fetch(src, dst):
-        copy = pltpu.make_async_copy(src, dst, local_sem.at[len(local)])
+    def fetch(src, dst, lot):
+        copy = pltpu.make_async_copy(src, dst, local_sem.at[lot])
         copy.start()
-        local.append(copy)
         return copy
 
-    got_tok = fetch(tokens, tok)
-    got_route = [fetch(ids, id_v), fetch(logits, lg), fetch(dense_mix, dmx)]
-    got_dense = [fetch(d_gate, dg), fetch(d_up, du)]
-    got_norm = [fetch(gain_mix, gm), fetch(w_ig, ig_w), fetch(w_fg, fg_w)]
+    got_tok = fetch(tokens, tok, 0)
+    got_route = [fetch(*p, 1) for p in ((ids, id_v), (logits, lg), (dense_mix, dmx))]
+    got_dense = [fetch(d_gate, dg, 2), fetch(d_up, du, 2)]
+    norm_in = ((gain_mix, gm), (w_ig, ig_w), (w_fg, fg_w), (norm_state, ns), (max_state, ms))
+    got_norm = [fetch(*p, 3) for p in norm_in]
     got_proj = [
-        fetch(w, wp.at[:, pl.ds(k * head, head)]) for k, w in enumerate((w_q, w_k, w_v, w_o))
+        fetch(w, wp.at[:, pl.ds(k * head, head)], 4) for k, w in enumerate((w_q, w_k, w_v, w_o))
     ]
-    got_cell = [fetch(cell, cs), fetch(norm_state, ns), fetch(max_state, ms)]
-    got_mix = fetch(w_mix, wm)
-    got_gf = fetch(gain_ffn, gf)
-    got_e = []
+    got_proj.append(fetch(cell, cs, 4))
+    got_late = [fetch(w_mix, wm, 5), fetch(gain_ffn, gf, 5)]
     for w, first, last in ((e_gate, 0, 2 * lead), (e_up, lead, 2 * lead + tail)):
         if lead:
-            got_e.append(fetch(w.at[0, pl.ds(0, lead)], egu.at[pl.ds(first, lead)]))
+            got_late.append(fetch(w.at[0, pl.ds(0, lead)], egu.at[pl.ds(first, lead)], 5))
         if ff > lead:
             rest = ff - lead
-            got_e.append(fetch(w.at[0, pl.ds(lead, rest)], egu.at[pl.ds(last, rest)]))
-    got_ed = fetch(e_down.at[0], ed)
-    got_dd = fetch(d_down, dd)
+            piece = w.at[0, pl.ds(lead, rest)]
+            got_late.append(fetch(piece, egu.at[pl.ds(last, rest)], 5))
+    got_late += [fetch(e_down.at[0], ed, 5), fetch(d_down, dd, 5)]
 
     def to_tp(src, dst, phase):
         for peer in peers:
@@ -201,15 +199,15 @@
 
     top, low = pl.ds(0, quarter // 2), pl.ds(quarter // 2, quarter // 2)
     far_top = bulk(pack.at[top], dgu.at[j, top], far, 0)
-    far_low = bulk(pack.at[low], dgu.at[j, low], far, 1)
-    near_gu = bulk(dgu.at[j], dgu.at[j], near, 2)
-    near_on = bulk(dgu.at[far], dgu.at[far], near, 3)
-    near_down = bulk(down_own, down.at[j // 2], near, 4)
-    cross_down = bulk(down_far, down.at[j // 2], cross, 5)
-    give_on = [bulk(give.at[g], take.at[g], near, 6 + g) for g in range(2)]
+    far_low = bulk(pack.at[low], dgu.at[j, low], far, 0)
+    near_gu = bulk(dgu.at[j], dgu.at[j], near, 1)
+    near_on = bulk(dgu.at[far], dgu.at[far], near, 2)
+    near_down = bulk(down_own, down.at[j // 2], near, 3)
+    cross_down = bulk(down_far, down.at[j // 2], cross, 4)
+    give_on = [bulk(give.at[g], take.at[g], near, 5 + g) for g in range(2)]
     blocks = [pl.ds(g * (n_half // 2), n_half // 2) for g in range(2)]
     res_on = [
-        bulk(res_all.at[other, b], res_all.at[other, b], near, 8 + g) for g, b in enumerate(blocks)
+        bulk(res_all.at[other, b], res_all.at[other, b], near, 7 + g) for g, b in enumerate(blocks)
     ]
 
     got_tok.wait()
@@ -267,6 +265,10 @@
     near_gu.start()
     for copy in got_norm:
         copy.wait()
+    @pl.when(core == 1)
+    def _():
+        pl.semaphore_wait(word_sem.at[0], lines)
+        signal(word_sem.at[1], (i + 2 * span - 4 * span * group, j))
     wait_bytes(tok_all, n_tp - 1, recv_sem.at[0])
     full = jnp.concatenate([tok_all[k] for k in range(n_tp)], axis=1).astype(F32)
     scale = lax.rsqrt(jnp.mean(full * full, axis=-1, keepdims=True) + EPS)
@@ -274,11 +276,10 @@
     normed_f = normed.astype(F32)
     ig = jnp.sum(normed_f * ig_w[...].astype(F32), axis=-1, keepdims=True)
     fg = jnp.sum(normed_f * fg_w[...].astype(F32), axis=-1, keepdims=True)
-
-    @pl.when(core == 1)
-    def _():
-        pl.semaphore_wait(word_sem.at[0], lines)
-        signal(word_sem.at[1], (i + 2 * span - 4 * span * group, j))
+    carried = jnp.minimum(fg, 0.0) - jnp.log1p(jnp.exp(-jnp.abs(fg))) + column(ms[...])
+    stab = jnp.maximum(carried, ig)
+    w_old = jnp.exp(carried - stab)
+    rise = jnp.exp(ig - stab)
     for copy in got_proj:
         copy.wait()
     proj = dot(normed, wp[...])
@@ -286,12 +287,7 @@
     key = proj[:, head : 2 * head] * head ** (-0.5)
     value = proj[:, 2 * head : 3 * head]
     out_gate = proj[:, 3 * head :]
-    for copy in got_cell:
-        copy.wait()
-    carried = jnp.minimum(fg, 0.0) - jnp.log1p(jnp.exp(-jnp.abs(fg))) + column(ms[...])
-    stab = jnp.maximum(carried, ig)
-    w_old = jnp.exp(carried - stab)
-    w_new = jnp.exp(ig - stab) * jnp.sum(query * key, axis=-1, keepdims=True)
+    w_new = rise * jnp.sum(query * key, axis=-1, keepdims=True)
     query_t = query.T
     for b in range(seq):
         read[b : b + 1, :] = jnp.sum(query_t[:, b : b + 1] * cs[b], axis=0, keepdims=True)
@@ -311,7 +307,8 @@
             signal(word_sem.at[2 + k], (f, j))
             pl.semaphore_wait(word_sem.at[2 + k], 1)
         signal(word_sem.at[2 + len(flips)], (i, near))
-    got_dd.wait()
+    for copy in got_late:
+        copy.wait()
     some = (down_own.shape[0], dff)
     to_row = lax.broadcasted_iota(jnp.int32, some, 0)
     from_row = lax.broadcasted_iota(jnp.int32, some, 1)
@@ -323,8 +320,6 @@
     down_own[...] = half_rows(j // 2)
     down_far[...] = half_rows(1 - j // 2)
     near_down.start()
-
-    got_mix.wait()
     wait_bytes(mix_all, n_tp - 1, recv_sem.at[3])
     heads = jnp.concatenate([mix_all[k] for k in range(n_tp)], axis=1)
     resid = (tok[...].astype(F32) + dot(heads, wm[...])).astype(BF16)
@@ -374,16 +369,16 @@
     lax.fori_loop(1, n_ep, send_rw, 0)
 
     across(send_res)
-    far_top.wait_recv()
-    far_low.wait_recv()
+    pltpu.make_async_copy(dgu.at[far], dgu.at[far], bulk_recv.at[0]).wait()
     near_on.start()
+    wait_bytes(dm_all, n_tp - 1, recv_sem.at[2])
+    tile = (quarter, quarter)
+    same = lax.broadcasted_iota(jnp.int32, tile, 0) == lax.broadcasted_iota(jnp.int32, tile, 1)
+    same = pick(same)
+    for q in range(n_tp):
+        turned[q] = dot_t(same, egu[:, q * quarter : (q + 1) * quarter]).astype(BF16)
     cross_down.start()
-    wait_bytes(dm_all, n_tp - 1, recv_sem.at[2])
-    got_gf.wait()
-    for copy in got_e:
-        copy.wait()
     near_gu.wait_recv()
-    got_ed.wait()
 
     lot = rows_all // 2
 
@@ -392,6 +387,10 @@
 
     def activated(g, u):
         return (g * jax.nn.sigmoid(g) * u).astype(BF16)
+
+    def arrived(g):
+        wait_bytes(res_all.at[other], n_half // 2, recv_sem.at[4 + 2 * g])
+        res_on[g].start()
 
     for g in range(2):
         def normalized(part):
@@ -406,17 +405,29 @@
             return cut, square, logit
 
         def expert_in(cut, part):
-            return sum(dot_t(cut[k], egu[:, columns(part, k)]) for k in range(half))
+            return sum(dot(cut[k], turned[2 * k + part]) for k in range(half))
 
         def dense_in(cut, part):
             return sum(dot(cut[k], dgu[2 * k + part]) for k in range(half))
-        wait_bytes(res_all.at[other], n_half // 2, recv_sem.at[4 + 2 * g])
-        res_on[g].start()
+        if g == 0:
+            arrived(0)
         cut_a, square_a, logit_a = normalized(other)
         expert_a = expert_in(cut_a, other)
         if g == 0:
             near_on.wait_recv()
         dense_a = dense_in(cut_a, other)
+        for here in range(2):
+
+            @pl.when(group == here)
+            def _():
+                wait_bytes(rw_all, n_ep // 2 - (here == g), recv_sem.at[1 + 6 * g])
+
+        wide = (n_ep // 2, seq, rw_all.shape[-1])
+        to_lane = lax.broadcasted_iota(jnp.int32, wide, 2)
+        diag = lax.broadcasted_iota(jnp.int32, wide, 1) == to_lane
+        mine_rw = rw_all[pl.ds(g * (n_ep // 2), n_ep // 2)]
+        some = jnp.where(diag, jnp.broadcast_to(mine_rw, wide), 0.0)
+        some = jnp.sum(some.reshape(lot, -1), axis=-1, keepdims=True)
         res_on[g].wait_recv()
         cut_b, square_b, logit_b = normalized(core)
         scale = lax.rsqrt((square_a + square_b) / (n_tp * quarter) + EPS)
@@ -430,18 +441,6 @@
             at = 2 * lead
             hidden.append(activated(mids[:, at : at + rest], mids[:, at + tail : at + tail + rest]))
         hidden = jnp.concatenate(hidden, axis=1)
-        for here in range(2):
-
-            @pl.when(group == here)
-            def _():
-                wait_bytes(rw_all, n_ep // 2 - (here == g), recv_sem.at[1 + 6 * g])
-
-        wide = (n_ep // 2, seq, rw_all.shape[-1])
-        to_lane = lax.broadcasted_iota(jnp.int32, wide, 2)
-        diag = lax.broadcasted_iota(jnp.int32, wide, 1) == to_lane
-        mine_rw = rw_all[pl.ds(g * (n_ep // 2), n_ep // 2)]
-        some = jnp.where(diag, jnp.broadcast_to(mine_rw, wide), 0.0)
-        some = jnp.sum(some.reshape(lot, -1), axis=-1, keepdims=True)
         def expert_part(part, k):
             return dot(hidden, ed[:, columns(part, k)]) * some
 
@@ -449,6 +448,8 @@
             give[g, k] = expert_part(core, k).astype(BF16).reshape(n_ep // 2, seq, quarter)
         give_on[g].start()
         kept = [expert_part(other, k) for k in range(half)]
+        if g == 0:
+            arrived(1)
         mids = (dense_a + dense_in(cut_b, core)) * scale
         middle = activated(mids[:, :mid], mids[:, mid : 2 * mid])
         if g == 0:
@@ -486,7 +487,8 @@
     wait_bytes(dm_all, n_tp - 1, send_sem.at[2])
     wait_bytes(mix_all, n_tp - 1, send_sem.at[3])
     wait_bytes(res_all.at[other], n_half, send_sem.at[4])
-    for copy in [far_top, far_low, near_gu, near_on, near_down, cross_down] + give_on + res_on:
+    pltpu.make_async_copy(pack, pack, bulk_send.at[0]).wait()
+    for copy in [near_gu, near_on, near_down, cross_down] + give_on + res_on:
         copy.wait_send()
     wait_bytes(c_in, n_half, send_sem.at[5])
     wait_bytes(c_in, n_half, recv_sem.at[5])
@@ -570,6 +572,7 @@
             pltpu.VMEM(w_mix_out.shape, BF16),
             pltpu.VMEM((seq, head, head), F32),
             pltpu.VMEM((wide, features), BF16),
+            pltpu.VMEM((n_tp, quarter, wide), BF16),
             pltpu.VMEM((ff, features), BF16),
             pltpu.VMEM((quarter, dff), BF16),
             pltpu.VMEM((quarter, dff), BF16),
@@ -593,11 +596,11 @@
             pltpu.VMEM((2, n_tp // 2, n_ep // 2, seq, quarter), BF16),
             pltpu.VMEM((n_tp // 2, n_ep, seq, quarter), BF16),
             pltpu.VMEM((n_all // 2, seq, quarter), BF16),
-            pltpu.SemaphoreType.DMA((24,)),
+            pltpu.SemaphoreType.DMA((N_LOCAL,)),
+            pltpu.SemaphoreType.DMA((6,)),
             pltpu.SemaphoreType.DMA((8,)),
-            pltpu.SemaphoreType.DMA((8,)),
-            pltpu.SemaphoreType.DMA((10,)),
-            pltpu.SemaphoreType.DMA((10,)),
+            pltpu.SemaphoreType.DMA((9,)),
+            pltpu.SemaphoreType.DMA((9,)),
             pltpu.SemaphoreType.REGULAR((n_ep.bit_length(),)),
         ],
         compiler_params=pltpu.CompilerParams(

time: 24.4 us -> 23.9 us (0.980)
  Pallas kernels: 23.6 us -> 23.1 us
    pallas_call x1, Pallas kernels: 23.6 us -> 23.1 us  [local(): pl.pallas_call(functools.partial(kernel, n_ep, n_tp), out_shape=pltpu.VME...]
where the time goes in v3:
time: 23.9 us; the launch traced here: 23.7 us
  Pallas kernels  23.1 us (97%)
  local copies, waits for them, and re-layouts  0.6 us (3%)
    pallas_call x1, Pallas kernels, local(): pl.pallas_call(functools.partial(kernel, n_ep, n_tp), out_shape=pltpu.VME...  23.1 us
    unnamed x1, local copies, waits for them, and re-layouts  0.6 us

profile of v3, /device:TPU:0, one launch (start us, length us, event | category | flops | bytes accessed | tf_op | source)
XLA Modules:
  0.0 23.7 jit_solution(14166913677223540177)
XLA Ops:
  0.0 23.1 %shard_map.208 = bf16[16,256]{1,0:T(8,128)(2,1)S(1)} custom-call(bf16[16,256]{1,0:T(8,128)(2,1)} %tokens.1, f32[1,1024]{1,0:T(1,128)} %bitcast.16, bf16[1,1024]{1,0:T(2,128)(2,1)} %bitcast.17, bf16[1,1024]{1,0:T(2,128)(2,1)} %bitcast.18, f32[16,128]{1,0:T(8,128)} %bitcast.15, f32[1,16]{1,0:T(1,128)} %bitcast.22, f32[1,1024]{1,0:T(1,128)} %bitcast.19, ...), custom_call_target="tpu_custom_call" | custom-call | tf_op jit(solution)/shard_map/pallas_call | solution.py:564
  23.1 0.6 %copy.24 = bf16[16,256]{1,0:T(8,128)(2,1)} copy(bf16[16,256]{1,0:T(8,128)(2,1)S(1)} %shard_map.208) | data formatting | bytes 16384

commit v4 on v3

--- a/solution.py
+++ b/solution.py
@@ -89,14 +89,15 @@
     res_own,
     res_all,
     read,
-    give,
-    take,
+    give_a,
+    give_b,
+    take_a,
+    take_b,
     c_out,
     c_in,
     local_sem,
     send_sem,
     recv_sem,
-    bulk_send,
     bulk_recv,
     word_sem,
 ):
@@ -120,7 +121,9 @@
     cross = lax.rem(near + 2, n_tp)
     span = n_ep // 4
     place = i // span
-    group = place // 2
+    group = jnp.minimum(place, 1)
+    edges = (0, span, n_ep)
+    counts = (span, n_ep - span)
 
     barrier = pltpu.get_barrier_semaphore()
     bits = [1 << k for k in reversed(range(n_ep.bit_length() - 3))]
@@ -177,7 +180,7 @@
             pltpu.make_async_remote_copy(
                 src_ref=src,
                 dst_ref=dst.at[j],
-                send_sem=send_sem.at[phase],
+                send_sem=send_sem.at[0],
                 recv_sem=recv_sem.at[phase],
                 device_id=peer,
                 device_id_type=MESH,
@@ -191,7 +194,7 @@
         return pltpu.make_async_remote_copy(
             src_ref=src,
             dst_ref=dst,
-            send_sem=bulk_send.at[k],
+            send_sem=send_sem.at[0],
             recv_sem=bulk_recv.at[k],
             device_id=(i, peer),
             device_id_type=MESH,
@@ -204,8 +207,9 @@
     near_on = bulk(dgu.at[far], dgu.at[far], near, 2)
     near_down = bulk(down_own, down.at[j // 2], near, 3)
     cross_down = bulk(down_far, down.at[j // 2], cross, 4)
-    give_on = [bulk(give.at[g], take.at[g], near, 5 + g) for g in range(2)]
-    blocks = [pl.ds(g * (n_half // 2), n_half // 2) for g in range(2)]
+    give, take = (give_a, give_b), (take_a, take_b)
+    give_on = [bulk(give[g], take[g], near, 5 + g) for g in range(2)]
+    blocks = [pl.ds(edges[g] * half, counts[g] * half) for g in range(2)]
     res_on = [
         bulk(res_all.at[other, b], res_all.at[other, b], near, 7 + g) for g, b in enumerate(blocks)
     ]
@@ -268,7 +272,7 @@
     @pl.when(core == 1)
     def _():
         pl.semaphore_wait(word_sem.at[0], lines)
-        signal(word_sem.at[1], (i + 2 * span - 4 * span * group, j))
+        signal(word_sem.at[1], (i + 2 * span - 4 * span * (place // 2), j))
     wait_bytes(tok_all, n_tp - 1, recv_sem.at[0])
     full = jnp.concatenate([tok_all[k] for k in range(n_tp)], axis=1).astype(F32)
     scale = lax.rsqrt(jnp.mean(full * full, axis=-1, keepdims=True) + EPS)
@@ -344,7 +348,7 @@
         pltpu.make_async_remote_copy(
             src_ref=res_own,
             dst_ref=res_all.at[core, mine],
-            send_sem=send_sem.at[4],
+            send_sem=send_sem.at[0],
             recv_sem=recv_sem.at[4 + 2 * group],
             device_id=(row, 2 * col + other),
             device_id_type=MESH,
@@ -359,7 +363,7 @@
         pltpu.make_async_remote_copy(
             src_ref=rw_own.at[e],
             dst_ref=rw_all.at[i],
-            send_sem=send_sem.at[1],
+            send_sem=send_sem.at[0],
             recv_sem=recv_sem.at[1 + 6 * group],
             device_id=(e, j),
             device_id_type=MESH,
@@ -380,7 +384,6 @@
     cross_down.start()
     near_gu.wait_recv()
 
-    lot = rows_all // 2
 
     def columns(part, k):
         return pl.ds(pl.multiple_of((2 * k + part) * quarter, quarter), quarter)
@@ -389,12 +392,15 @@
         return (g * jax.nn.sigmoid(g) * u).astype(BF16)
 
     def arrived(g):
-        wait_bytes(res_all.at[other], n_half // 2, recv_sem.at[4 + 2 * g])
+        wait_bytes(res_all.at[other], counts[g] * half, recv_sem.at[4 + 2 * g])
         res_on[g].start()
 
     for g in range(2):
+        n_rows = counts[g]
+        lot = n_rows * seq
+
         def normalized(part):
-            rows = res_all[part, blocks[g]].reshape(n_ep // 2, half, seq, quarter)
+            rows = res_all[part, blocks[g]].reshape(n_rows, half, seq, quarter)
             cut, square, logit = [], 0.0, 0.0
             for k in range(half):
                 block = rows[:, k].reshape(lot, quarter).astype(F32)
@@ -420,12 +426,12 @@
 
             @pl.when(group == here)
             def _():
-                wait_bytes(rw_all, n_ep // 2 - (here == g), recv_sem.at[1 + 6 * g])
-
-        wide = (n_ep // 2, seq, rw_all.shape[-1])
+                wait_bytes(rw_all, n_rows - (here == g), recv_sem.at[1 + 6 * g])
+
+        wide = (n_rows, seq, rw_all.shape[-1])
         to_lane = lax.broadcasted_iota(jnp.int32, wide, 2)
         diag = lax.broadcasted_iota(jnp.int32, wide, 1) == to_lane
-        mine_rw = rw_all[pl.ds(g * (n_ep // 2), n_ep // 2)]
+        mine_rw = rw_all[pl.ds(edges[g], n_rows)]
         some = jnp.where(diag, jnp.broadcast_to(mine_rw, wide), 0.0)
         some = jnp.sum(some.reshape(lot, -1), axis=-1, keepdims=True)
         res_on[g].wait_recv()
@@ -445,11 +451,9 @@
             return dot(hidden, ed[:, columns(part, k)]) * some
 
         for k in range(half):
-            give[g, k] = expert_part(core, k).astype(BF16).reshape(n_ep // 2, seq, quarter)
+            give[g][k] = expert_part(core, k).astype(BF16).reshape(n_rows, seq, quarter)
         give_on[g].start()
         kept = [expert_part(other, k) for k in range(half)]
-        if g == 0:
-            arrived(1)
         mids = (dense_a + dense_in(cut_b, core)) * scale
         middle = activated(mids[:, :mid], mids[:, mid : 2 * mid])
         if g == 0:
@@ -459,38 +463,32 @@
             kept[k] += dot(middle, down[k, 0:mid]) * mix_gate
         give_on[g].wait_recv()
         for k in range(half):
-            total = kept[k] + take[g, k].reshape(lot, quarter).astype(F32)
-            c_out[k, pl.ds(g * (n_ep // 2), n_ep // 2)] = total.astype(BF16).reshape(
-                n_ep // 2, seq, quarter
-            )
-        first = jnp.where(group == g, 1, 0)
-
-        def send_back(t, carry):
-            high = g * (ring // 2) + lax.rem(i // 2 + first + t, ring // 2)
-            for down_y in (1, 0):
-                row = 2 * high + lax.rem(i + down_y, 2)
-                for step in reversed(range(half)):
-                    col = lax.rem(j // 2 + step, half)
-                    pltpu.make_async_remote_copy(
-                        src_ref=c_out.at[col, row],
-                        dst_ref=c_in.at[mine],
-                        send_sem=send_sem.at[5],
-                        recv_sem=recv_sem.at[5],
-                        device_id=(row, 2 * col + other),
-                        device_id_type=MESH,
-                    ).start()
+            total = kept[k] + take[g][k].reshape(lot, quarter).astype(F32)
+            c_out[k, pl.ds(edges[g], n_rows)] = total.astype(BF16).reshape(n_rows, seq, quarter)
+        def send_back(row, carry):
+            for col in range(half):
+                pltpu.make_async_remote_copy(
+                    src_ref=c_out.at[col, row],
+                    dst_ref=c_in.at[mine],
+                    send_sem=send_sem.at[0],
+                    recv_sem=recv_sem.at[5],
+                    device_id=(row, 2 * col + other),
+                    device_id_type=MESH,
+                ).start()
             return carry
 
-        lax.fori_loop(0, ring // 2, send_back, 0, unroll=ring <= 4)
+        lax.fori_loop(edges[g], edges[g + 1], send_back, 0, unroll=n_ep <= 8)
+        if g == 0:
+            arrived(1)
     wait_bytes(tok_all, n_tp - 1, send_sem.at[0])
-    wait_bytes(rw_all, n_ep - 1, send_sem.at[1])
-    wait_bytes(dm_all, n_tp - 1, send_sem.at[2])
-    wait_bytes(mix_all, n_tp - 1, send_sem.at[3])
-    wait_bytes(res_all.at[other], n_half, send_sem.at[4])
-    pltpu.make_async_copy(pack, pack, bulk_send.at[0]).wait()
+    wait_bytes(rw_all, n_ep - 1, send_sem.at[0])
+    wait_bytes(dm_all, n_tp - 1, send_sem.at[0])
+    wait_bytes(mix_all, n_tp - 1, send_sem.at[0])
+    wait_bytes(res_all.at[other], n_half, send_sem.at[0])
+    pltpu.make_async_copy(pack, pack, send_sem.at[0]).wait()
     for copy in [near_gu, near_on, near_down, cross_down] + give_on + res_on:
         copy.wait_send()
-    wait_bytes(c_in, n_half, send_sem.at[5])
+    wait_bytes(c_in, n_half, send_sem.at[0])
     wait_bytes(c_in, n_half, recv_sem.at[5])
     def add(k, total):
         return total + c_in[k].astype(F32)
@@ -592,14 +590,15 @@
             pltpu.VMEM((seq, quarter), BF16),
             pltpu.VMEM((2, n_all // 2, seq, quarter), BF16),
             pltpu.VMEM((seq, head), F32),
-            pltpu.VMEM((2, n_tp // 2, n_ep // 2, seq, quarter), BF16),
-            pltpu.VMEM((2, n_tp // 2, n_ep // 2, seq, quarter), BF16),
+            pltpu.VMEM((n_tp // 2, n_ep // 4, seq, quarter), BF16),
+            pltpu.VMEM((n_tp // 2, n_ep - n_ep // 4, seq, quarter), BF16),
+            pltpu.VMEM((n_tp // 2, n_ep // 4, seq, quarter), BF16),
+            pltpu.VMEM((n_tp // 2, n_ep - n_ep // 4, seq, quarter), BF16),
             pltpu.VMEM((n_tp // 2, n_ep, seq, quarter), BF16),
             pltpu.VMEM((n_all // 2, seq, quarter), BF16),
             pltpu.SemaphoreType.DMA((N_LOCAL,)),
-            pltpu.SemaphoreType.DMA((6,)),
+            pltpu.SemaphoreType.DMA((1,)),
             pltpu.SemaphoreType.DMA((8,)),
-            pltpu.SemaphoreType.DMA((9,)),
             pltpu.SemaphoreType.DMA((9,)),
             pltpu.SemaphoreType.REGULAR((n_ep.bit_length(),)),
         ],

time: 23.9 us -> 22.8 us (0.954)
  Pallas kernels: 23.1 us -> 21.8 us
    pallas_call x1, Pallas kernels: 23.1 us -> 21.8 us  [local(): pl.pallas_call(functools.partial(kernel, n_ep, n_tp), out_shape=pltpu.VME...]
where the time goes in v4:
time: 22.8 us; the launch traced here: 22.4 us
  Pallas kernels  21.8 us (96%)
  local copies, waits for them, and re-layouts  0.6 us (3%)
    pallas_call x1, Pallas kernels, local(): pl.pallas_call(functools.partial(kernel, n_ep, n_tp), out_shape=pltpu.VME...  21.8 us
    unnamed x1, local copies, waits for them, and re-layouts  0.6 us

profile of v4, /device:TPU:0, one launch (start us, length us, event | category | flops | bytes accessed | tf_op | source)
XLA Modules:
  0.0 22.4 jit_solution(1526311126461931430)
XLA Ops:
  0.0 21.8 %shard_map.208 = bf16[16,256]{1,0:T(8,128)(2,1)S(1)} custom-call(bf16[16,256]{1,0:T(8,128)(2,1)} %tokens.1, f32[1,1024]{1,0:T(1,128)} %bitcast.16, bf16[1,1024]{1,0:T(2,128)(2,1)} %bitcast.17, bf16[1,1024]{1,0:T(2,128)(2,1)} %bitcast.18, f32[16,128]{1,0:T(8,128)} %bitcast.15, f32[1,16]{1,0:T(1,128)} %bitcast.22, f32[1,1024]{1,0:T(1,128)} %bitcast.19, ...), custom_call_target="tpu_custom_call" | custom-call | tf_op jit(solution)/shard_map/pallas_call | solution.py:562
  21.8 0.6 %copy.24 = bf16[16,256]{1,0:T(8,128)(2,1)} copy(bf16[16,256]{1,0:T(8,128)(2,1)S(1)} %shard_map.208) | data formatting | bytes 16384
